TPU v7x, 32 devices: a whole 2x2x4 slice. The times are simulated.
32 devices in a mesh: sp: 16 (over z, y, x), tp: 2 (over core).
Axes of the slice: x: 2, y: 2, z: 4, core: 2. Of those that a mesh axis runs over, the one named last changes fastest.
Arguments:
- queries: bfloat16 [4096, 1024], P('sp', 'tp'), may hold values from -6 to 6
- keys: bfloat16 [4096, 256], P('sp'), may hold values from -6 to 6
- values: bfloat16 [4096, 256], P('sp'), may hold values from -6 to 6
- query_gain: float32 [128], replicated, may hold values from 1.4 to 5.5
- key_gain: float32 [128], replicated, may hold values from 1.4 to 5.5
- residual_in: bfloat16 [4096, 2048], P(('sp', 'tp')), may hold values from -6 to 6
- out_weight: bfloat16 [1024, 2048], P('tp'), may hold values from -0.1875 to 0.1875
- norm_gain: float32 [2048], replicated, may hold values from 0.1 to 1.9
- gate_weight: bfloat16 [2048, 3072], P('sp', 'tp'), may hold values from -0.125 to 0.125
- up_weight: bfloat16 [2048, 3072], P('sp', 'tp'), may hold values from -0.125 to 0.125
- down_weight: bfloat16 [3072, 2048], P('tp', 'sp'), may hold values from -0.109375 to 0.109375
Outputs:
- result: bfloat16 [4096, 2048], P(('sp', 'tp'))
All inputs are finite; a program needn't handle non-finite values.
Results may differ from a plain program's by a relative error of at most 0.017.
Values may be sent and summed in bfloat16 or wider, within the bound.
A program may use at most 64 MiB of HBM per device.

v0:
```python
import math
import jax
import jax.numpy as jnp
from jax import lax
from jax.sharding import PartitionSpec as P

Q_HEADS = 8
KV_HEADS = 2
GRID_WIDTH = 64
EPS = 1e-06
ROPE_BASE = 10000.0


def normalize(wide_values, gain):
    wide = wide_values.astype(jnp.float32)
    return wide * lax.rsqrt(jnp.mean(wide * wide, axis=-1, keepdims=True) + EPS) * gain


def rotate_pair(segment, angles):
    half_size = segment.shape[-1] // 2
    first = segment[..., :half_size]
    second = segment[..., half_size:]
    cosine = jnp.cos(angles)[:, None, :]
    sine_part = jnp.sin(angles)[:, None, :]
    return jnp.concatenate(
        [first * cosine - second * sine_part, second * cosine + first * sine_part], axis=-1
    )


def grid_rotary(head_rows, positions):
    head_size = head_rows.shape[-1]
    half_size = head_size // 2
    quarter = head_size // 4
    inverse = ROPE_BASE ** (-jnp.arange(quarter, dtype=jnp.float32) * 2.0 / half_size)
    row_angles = (positions // GRID_WIDTH).astype(jnp.float32)[:, None] * inverse
    col_angles = (positions % GRID_WIDTH).astype(jnp.float32)[:, None] * inverse
    return jnp.concatenate(
        [
            rotate_pair(head_rows[..., :half_size], row_angles),
            rotate_pair(head_rows[..., half_size:], col_angles),
        ],
        axis=-1,
    )


def gated(gate_part, lifted):
    return (jax.nn.silu(gate_part) * lifted).astype(jnp.bfloat16)


def local(
    queries,
    keys,
    values,
    query_gain,
    key_gain,
    residual_in,
    out_weight,
    norm_gain,
    gate_weight,
    up_weight,
    down_weight,
):
    tok_rows = queries.shape[0]
    head_size = query_gain.shape[0]
    local_heads = queries.shape[1] // head_size
    tp_index = lax.axis_index("tp")
    share = tok_rows // lax.axis_size("tp")
    positions = lax.axis_index("sp") * tok_rows + jnp.arange(tok_rows, dtype=jnp.int32)
    key_head = tp_index * local_heads // (Q_HEADS // KV_HEADS)
    own_keys = lax.dynamic_slice_in_dim(keys, key_head * head_size, head_size, 1)
    own_values = lax.dynamic_slice_in_dim(values, key_head * head_size, head_size, 1)
    turned_keys = grid_rotary(
        normalize(own_keys.reshape(tok_rows, 1, head_size), key_gain), positions
    )
    turned_keys = turned_keys.reshape(tok_rows, head_size).astype(jnp.bfloat16)
    turned_queries = grid_rotary(
        normalize(queries.reshape(tok_rows, local_heads, head_size), query_gain), positions
    )
    turned_queries = turned_queries.reshape(tok_rows * local_heads, head_size).astype(jnp.bfloat16)
    score_scale = head_size ** (-0.5)

    def attend_block(running, block_pair):
        peak_score, weight_total, weighted = running
        block_keys, block_values = block_pair
        scores = (
            lax.dot_general(
                turned_queries,
                block_keys,
                (((1,), (1,)), ((), ())),
                preferred_element_type=jnp.float32,
            )
            * score_scale
        )
        new_peak = jnp.maximum(peak_score, jnp.max(scores, axis=1))
        factor = jnp.exp(peak_score - new_peak)
        raw = jnp.exp(scores - new_peak[:, None])
        weight_total = weight_total * factor + jnp.sum(raw, axis=1)
        weighted = weighted * factor[:, None] + jnp.dot(
            raw.astype(jnp.bfloat16), block_values, preferred_element_type=jnp.float32
        )
        return ((new_peak, weight_total, weighted), None)

    row_count = tok_rows * local_heads
    start_carry = (
        jnp.full((row_count,), -1e30, jnp.float32),
        jnp.zeros((row_count,), jnp.float32),
        jnp.zeros((row_count, head_size), jnp.float32),
    )
    piece_keys = lax.all_gather(turned_keys, "sp", axis=0, tiled=True)
    piece_values = lax.all_gather(own_values, "sp", axis=0, tiled=True)
    span = math.gcd(piece_keys.shape[0], 512)
    blocks = piece_keys.shape[0] // span
    stacked = (
        piece_keys.reshape(blocks, span, head_size),
        piece_values.reshape(blocks, span, head_size),
    )
    updated, unused = lax.scan(attend_block, start_carry, stacked)
    peak_score, weight_total, weighted = updated
    attended = (
        (weighted / weight_total[:, None])
        .astype(jnp.bfloat16)
        .reshape(tok_rows, local_heads * head_size)
    )
    placed = lax.dynamic_update_slice_in_dim(
        jnp.zeros((tok_rows, residual_in.shape[1]), jnp.float32),
        residual_in.astype(jnp.float32),
        tp_index * share,
        0,
    )
    head_partial = jnp.dot(attended, out_weight, preferred_element_type=jnp.float32)
    partial_total, residual_rows = (
        lax.psum(head_partial.astype(jnp.bfloat16), "tp").astype(jnp.float32),
        lax.psum(placed.astype(jnp.bfloat16), "tp").astype(jnp.float32),
    )
    middle_rows = (residual_rows + partial_total).astype(jnp.bfloat16)
    normed = normalize(middle_rows, norm_gain).astype(jnp.bfloat16)
    middle = lax.dynamic_slice_in_dim(middle_rows, tp_index * share, share, 0)
    hidden_width = gate_weight.shape[1]
    side_by_side = jnp.concatenate(
        [
            lax.all_gather(gate_weight, "sp", axis=0, tiled=True),
            lax.all_gather(up_weight, "sp", axis=0, tiled=True),
        ],
        axis=1,
    )
    both_parts = jnp.dot(normed, side_by_side, preferred_element_type=jnp.float32)
    hidden = gated(both_parts[:, :hidden_width], both_parts[:, hidden_width:])
    partials = jnp.dot(
        hidden,
        lax.all_gather(down_weight, "sp", axis=1, tiled=True),
        preferred_element_type=jnp.float32,
    )
    mixer_out = lax.psum_scatter(
        partials.astype(jnp.bfloat16), "tp", scatter_dimension=0, tiled=True
    ).astype(jnp.float32)
    return (middle.astype(jnp.float32) + mixer_out).astype(jnp.bfloat16)


def solution(mesh):
    return jax.shard_map(
        local,
        mesh=mesh,
        in_specs=(
            P("sp", "tp"),
            P("sp", None),
            P("sp", None),
            P(),
            P(),
            P(("sp", "tp"), None),
            P("tp", None),
            P(),
            P("sp", "tp"),
            P("sp", "tp"),
            P("tp", "sp"),
        ),
        out_specs=P(("sp", "tp"), None),
        check_vma=False,
    )
```

profile of v0, /device:TPU:0, one launch (start us, length us, event | category | flops | bytes accessed | tf_op | source)
XLA Modules:
  0.0 528.7 jit_solution(11063251506600256293)
XLA Ops:
  6.6 1.0 constant_dynamic-slice_fusion.1
  7.6 0.1 copy.20
  7.7 0.7 fusion.29
  8.5 0.3 fusion.43
  8.8 0.6 pad_maximum_fusion.1
  9.5 1.5 constant_dynamic-slice_fusion
  11.1 1.1 reshape.287
  12.2 0.3 multiply_reduce_fusion.1
  12.6 1.0 multiply_cosine_fusion.1
  13.6 0.3 multiply_multiply_fusion
  13.9 0.9 subtract_convert_fusion.1
  14.9 0.8 pad_maximum_fusion
  15.7 1.1 broadcast_in_dim.8
  16.8 0.9 convert_dynamic-update-slice_fusion
  17.7 50.1 %all-gather.15.cloned.1.call-done = bf16[4096,1,128]{0,2,1:T(8,128)(2,1)} async-done(((bf16[256,1,128]{0,2,1:T(8,128)(2,1)}), bf16[4096,1,128]{0,2,1:T(8,128)(2,1)}) %all-gather.15.cloned.1.call-update) | async-done | bytes 1048592 | tf_op jit(solution)/shard_map/all_gather | solution.py:109
  67.8 2.3 copy.19
  70.1 54.3 %all-gather.7.cloned.1.call-done = bf16[4096,128]{1,0:T(8,128)(2,1)} async-done(((bf16[256,128]{1,0:T(8,128)(2,1)}), bf16[4096,128]{1,0:T(8,128)(2,1)}) %all-gather.7.cloned.1.call-update) | async-done | bytes 1048592 | tf_op jit(solution)/shard_map/all_gather | solution.py:110
  124.4 51.7 %while.15 = (s32[]{:T(128)}, f32[1024]{0:T(1024)S(1)}, f32[1024]{0:T(1024)S(1)}, f32[1024,128]{1,0:T(8,128)S(1)}, bf16[8,512,128]{2,1,0:T(8,128)(2,1)}, /*index=...) while((s32[]{:T(128)}, f32[1024]{0:T(1024)S(1)}, ...), condition=%wide.region_6.7_spmd.clone, body=%wide.region_3.6_spmd.clone.sunk | while | flops 273028096 | bytes 16319621 | solution.py:117
  124.4 2.7 multiply_reduce_fusion.3
  127.0 2.1 fusion.63
  129.2 0.1 copy-done.1
  129.3 1.5 convolution_add_fusion.2
  130.8 2.7 multiply_reduce_fusion.3
  133.5 2.1 fusion.63
  135.6 0.1 copy-done.1
  135.7 1.5 convolution_add_fusion.2
  137.3 2.7 multiply_reduce_fusion.3
  140.0 2.1 fusion.63
  142.1 0.1 copy-done.1
  142.2 1.5 convolution_add_fusion.2
  143.7 2.7 multiply_reduce_fusion.3
  146.4 2.1 fusion.63
  148.5 0.1 copy-done.1
  148.6 1.5 convolution_add_fusion.2
  150.2 2.7 multiply_reduce_fusion.3
  152.9 2.1 fusion.63
  155.0 0.1 copy-done.1
  155.1 1.5 convolution_add_fusion.2
  156.7 2.7 multiply_reduce_fusion.3
  159.3 2.1 fusion.63
  161.5 0.1 copy-done.1
  161.6 1.5 convolution_add_fusion.2
  163.1 2.7 multiply_reduce_fusion.3
  165.8 2.1 fusion.63
  167.9 0.1 copy-done.1
  168.0 1.5 convolution_add_fusion.2
  169.6 2.7 multiply_reduce_fusion.3
  172.3 2.1 fusion.63
  174.5 1.5 convolution_add_fusion.2
  176.0 0.2 divide_convert_fusion
  176.2 0.2 reshape.286
  176.4 1.7 convolution_convert_fusion
  178.2 0.5 all-gather.11.cloned.1.call-update
  178.8 0.5 all-gather.9.cloned.1.call-update
  179.4 0.5 all-gather.13.cloned.1.call-update
  179.9 18.6 %all-reduce.3.cloned.1.call-done = (bf16[256,2048]{1,0:T(8,128)(2,1)}, bf16[256,2048]{1,0:T(8,128)(2,1)}) async-done(((bf16[256,2048]{1,0:T(8,128)(2,1)}, bf16[256,2048]{1,0:T(8,128)(2,1)}), (bf16[256,2048]{1,0:T(8,128)(2,1)}, bf16[256,2048]{1,0:T(8,128)(2,1)})) %all-reduce.3.cloned.1.call-update) | async-done | bytes 2097168 | tf_op jit(solution)/shard_map/psum | solution.py:132
  198.5 2.0 fusion.18
  200.6 95.2 %all-gather.11.cloned.1.call-done = bf16[2048,1536]{1,0:T(8,128)(2,1)} async-done(((bf16[128,1536]{1,0:T(8,128)(2,1)}), bf16[2048,1536]{1,0:T(8,128)(2,1)}) %all-gather.11.cloned.1.call-update) | async-done | bytes 6291472 | tf_op jit(solution)/shard_map/all_gather | solution.py:142
  295.8 94.6 %all-gather.9.cloned.1.call-done = bf16[2048,1536]{1,0:T(8,128)(2,1)} async-done(((bf16[128,1536]{1,0:T(8,128)(2,1)}), bf16[2048,1536]{1,0:T(8,128)(2,1)}) %all-gather.9.cloned.1.call-update) | async-done | bytes 6291472 | tf_op jit(solution)/shard_map/all_gather | solution.py:141
  390.4 9.8 %fusion.14 = f32[256,3072]{1,0:T(8,128)} fusion(bf16[2048,1536]{1,0:T(8,128)(2,1)} %all-gather.11.cloned.1.call-done, bf16[2048,1536]{1,0:T(8,128)(2,1)} %all-gather.9.cloned.1.call-done, bf16[256,2048]{1,0:T(8,128)(2,1)S(1)} %get-tuple-element.102, f32[2048]{0:T(1024)S(1)} %copy-done.4, f32[256]{0:T(256)S(1)} %add_rsqrt_fusion.1), kind=kOutput, calls=%fused_computation.20 | convolution fusion | flops 3248488448 | bytes 16786432 | tf_op jit(solution)/shard_map/dot_general | solution.py:146
  400.2 106.3 %all-gather.13.cloned.1.call-done = bf16[1536,2048]{1,0:T(8,128)(2,1)} async-done(((bf16[1536,128]{1,0:T(8,128)(2,1)}), bf16[1536,2048]{1,0:T(8,128)(2,1)}) %all-gather.13.cloned.1.call-update) | async-done | bytes 6291472 | tf_op jit(solution)/shard_map/all_gather | solution.py:150
  506.5 6.6 %convolution_convert_fusion.1 = bf16[256,2048]{1,0:T(8,128)(2,1)} fusion(bf16[1536,2048]{1,0:T(8,128)(2,1)} %all-gather.13.cloned.1.call-done, f32[256,3072]{1,0:T(8,128)} %fusion.14), kind=kOutput, calls=%fused_computation.27 | convolution fusion | flops 1613496320 | bytes 10485760 | tf_op jit(solution)/shard_map/dot_general | solution.py:148
  513.1 6.7 %reduce-scatter.2.cloned.1.call-done = bf16[128,2048]{1,0:T(8,128)(2,1)} async-done(((bf16[256,2048]{1,0:T(8,128)(2,1)}), bf16[128,2048]{1,0:T(8,128)(2,1)}) %reduce-scatter.2.cloned.1.call-update) | async-done | bytes 524304 | tf_op jit(solution)/shard_map/reduce_scatter | solution.py:153
  519.9 2.0 add_convert_fusion.1
  (61 shorter events, 0.7 us)
Async XLA Ops:
  6.5 169.9 %copy-start = (bf16[512,2048]{1,0:T(8,128)(2,1)S(1)}, bf16[512,2048]{1,0:T(8,128)(2,1)}, u32[]{:S(2)}) copy-start(bf16[512,2048]{1,0:T(8,128)(2,1)} %param.19) | copy-start | bytes 6291460
  6.5 7.1 %copy-start.3 = (f32[128]{0:T(128)S(1)}, f32[128]{0:T(128)}, u32[]{:S(2)}) copy-start(f32[128]{0:T(128)} %param.16) | copy-start | bytes 1540
  6.5 61.3 %all-gather.15.cloned.1.call-start = ((), (), s32[]{:S(2)}) async-start(), calls=%async_computation.6 | async-start | bytes 1114112 | tf_op jit(solution)/shard_map/all_gather | solution.py:109
  9.5 114.9 %all-gather.7.cloned.1.call-start = ((), (), s32[]{:S(2)}) async-start(), calls=%async_computation.1 | async-start | bytes 1114112 | tf_op jit(solution)/shard_map/all_gather | solution.py:110
  11.0 187.5 %all-reduce.3.cloned.1.call-start = ((), (), s32[]{:S(2)}) async-start(), calls=%async_computation.7 | async-start | bytes 4194304 | tf_op jit(solution)/shard_map/psum | solution.py:132
  14.8 2.0 copy-start.2
  127.0 2.2 copy-start.1
  133.5 2.2 copy-start.1
  140.0 2.2 copy-start.1
  146.4 2.2 copy-start.1
  152.9 2.2 copy-start.1
  159.3 2.2 copy-start.1
  165.8 2.2 copy-start.1
  172.3 2.2 copy-start.1
  178.1 212.2 %copy-start.4 = (f32[2048]{0:T(1024)S(1)}, f32[2048]{0:T(1024)}, u32[]{:S(2)}) copy-start(f32[2048]{0:T(1024)} %param.20) | copy-start | bytes 24580
  178.1 117.6 %all-gather.11.cloned.1.call-start = ((), (), s32[]{:S(2)}) async-start(), calls=%async_computation.3 | async-start | bytes 6684672 | tf_op jit(solution)/shard_map/all_gather | solution.py:142
  178.7 211.6 %all-gather.9.cloned.1.call-start = ((), (), s32[]{:S(2)}) async-start(), calls=%async_computation.2 | async-start | bytes 6684672 | tf_op jit(solution)/shard_map/all_gather | solution.py:141
  179.3 327.2 %all-gather.13.cloned.1.call-start = ((), (), s32[]{:S(2)}) async-start(), calls=%async_computation.4 | async-start | bytes 6684672 | tf_op jit(solution)/shard_map/all_gather | solution.py:150
  179.9 340.0 %reduce-scatter.2.cloned.1.call-start = ((), (), s32[]{:S(2)}) async-start(), calls=%async_computation.5 | async-start | bytes 1572864 | tf_op jit(solution)/shard_map/reduce_scatter | solution.py:153
Sparse Core Ops, SparseCore 0:
  10.1 57.6 all-gather.14
  70.6 53.7 all-gather.6
  178.3 20.2 all-reduce.2
  201.1 94.5 all-gather.10
  298.4 91.9 all-gather.8
  392.9 113.5 all-gather.12
  513.2 6.5 reduce-scatter.1
where the time goes:
time: 529 us
  waiting for transfers between devices  428 us (81%)
  matrix products  51.7 us (10%)
  other arithmetic  27.3 us (5%)
  between operations  13.7 us (3%)
  local copies, waits for them, and re-layouts  8.01 us (2%)
    all_gather x1, waiting for transfers between devices, local(): lax.all_gather(down_weight, 'sp', axis=1, tiled=True)  106 us
    all_gather x1, waiting for transfers between devices, local(): lax.all_gather(up_weight, 'sp', axis=0, tiled=True)  95.2 us
    all_gather x1, waiting for transfers between devices, local(): lax.all_gather(gate_weight, 'sp', axis=0, tiled=True)  94.6 us
    all_gather x1, waiting for transfers between devices, local(): piece_values = lax.all_gather(own_values, 'sp', axis=0, tiled=True)  54.3 us
    all_gather x1, waiting for transfers between devices, local(): piece_keys = lax.all_gather(turned_keys, 'sp', axis=0, tiled=True)  50.1 us
    dot_general x8, matrix products, attend_block(): lax.dot_general(turned_queries, block_keys, (((1,), (1,)), ((), ())), pre...  21.4 us
    psum x1, waiting for transfers between devices, local(): lax.psum(head_partial.astype(jnp.bfloat16), 'tp').astype(jnp.float32)  18.6 us
    reduce_sum x8, other arithmetic, attend_block(): weight_total = weight_total * factor + jnp.sum(raw, axis=1)  16.9 us
  transfers between devices with their start and end apart: 7, of which 7 were waited for; matrix products, arithmetic and copies ran while one was open for 4% of the time, Pallas kernels for 0%

commit v1 on v0

--- a/solution.py
+++ b/solution.py
@@ -106,8 +106,13 @@
         jnp.zeros((row_count,), jnp.float32),
         jnp.zeros((row_count, head_size), jnp.float32),
     )
-    piece_keys = lax.all_gather(turned_keys, "sp", axis=0, tiled=True)
-    piece_values = lax.all_gather(own_values, "sp", axis=0, tiled=True)
+    piece_keys, piece_values = jnp.split(
+        lax.all_gather(
+            jnp.concatenate([turned_keys, own_values], axis=1), "sp", axis=0, tiled=True
+        ),
+        [turned_keys.shape[1]],
+        axis=1,
+    )
     span = math.gcd(piece_keys.shape[0], 512)
     blocks = piece_keys.shape[0] // span
     stacked = (

time: 529 us -> 490 us (0.926)
  waiting for transfers between devices: 428 us -> 384 us
    all_gather x2 -> x1, waiting for transfers between devices: 104 us -> 61.2 us  [local(): lax.all_gather(jnp.concatenate([turned_keys, own_values], axis=1), 'sp',...]
  transfers between devices with their start and end apart: 7 -> 6, of which waited for: 7 -> 6; matrix products, arithmetic and copies ran while one was open for 4% -> 4% of each run, Pallas kernels for 0% -> 0%
where the time goes in v1:
time: 490 us; the launch traced here: 489 us
  waiting for transfers between devices  384 us (78%)
  matrix products  51.8 us (11%)
  other arithmetic  27.3 us (6%)
  between operations  13.7 us (3%)
  local copies, waits for them, and re-layouts  12.1 us (2%)
    all_gather x1, waiting for transfers between devices, local(): lax.all_gather(down_weight, 'sp', axis=1, tiled=True)  106 us
    all_gather x1, waiting for transfers between devices, local(): lax.all_gather(gate_weight, 'sp', axis=0, tiled=True)  95.3 us
    all_gather x1, waiting for transfers between devices, local(): lax.all_gather(up_weight, 'sp', axis=0, tiled=True)  94.6 us
    all_gather x1, waiting for transfers between devices, local(): lax.all_gather(jnp.concatenate([turned_keys, own_values], axis=1), 'sp',...  61.2 us
    dot_general x8, matrix products, attend_block(): lax.dot_general(turned_queries, block_keys, (((1,), (1,)), ((), ())), pre...  21.4 us
    psum x1, waiting for transfers between devices, local(): lax.psum(head_partial.astype(jnp.bfloat16), 'tp').astype(jnp.float32)  17.8 us
    reduce_sum x8, other arithmetic, attend_block(): weight_total = weight_total * factor + jnp.sum(raw, axis=1)  16.9 us
    dot_general x8, matrix products, attend_block(): jnp.dot(raw.astype(jnp.bfloat16), block_values, preferred_element_type=jn...  12.3 us
  transfers between devices with their start and end apart: 6, of which 6 were waited for; matrix products, arithmetic and copies ran while one was open for 4% of the time, Pallas kernels for 0%

profile of v1, /device:TPU:0, one launch (start us, length us, event | category | flops | bytes accessed | tf_op | source)
XLA Modules:
  0.0 489.3 jit_solution(2148835658528029041)
XLA Ops:
  6.6 1.0 constant_dynamic-slice_fusion
  7.6 0.1 copy.25
  7.8 0.1 copy.26
  7.9 0.7 fusion.29
  8.6 0.3 fusion.43
  9.0 0.7 pad_maximum_fusion.1
  9.8 1.1 reshape.287
  10.9 0.3 multiply_reduce_fusion.1
  11.3 1.0 multiply_cosine_fusion.1
  12.3 0.3 multiply_multiply_fusion
  12.6 0.9 subtract_convert_fusion.1
  13.5 0.8 pad_maximum_fusion
  14.3 1.1 broadcast_in_dim.8
  15.5 0.9 convert_dynamic-update-slice_fusion
  16.3 61.2 %all-gather.5.cloned.1.call-done = bf16[4096,256]{0,1:T(8,128)(2,1)} async-done(((bf16[256,256]{0,1:T(8,128)(2,1)}), bf16[4096,256]{0,1:T(8,128)(2,1)}) %all-gather.5.cloned.1.call-update) | async-done | bytes 2097168 | tf_op jit(solution)/shard_map/all_gather | solution.py:110
  77.5 3.1 fusion.51
  80.7 2.3 copy.23
  82.9 2.3 copy.24
  85.2 51.7 %while.15 = (s32[]{:T(128)}, f32[1024]{0:T(1024)S(1)}, f32[1024]{0:T(1024)S(1)}, f32[1024,128]{1,0:T(8,128)S(1)}, bf16[8,512,128]{2,1,0:T(8,128)(2,1)}, /*index=...) while((s32[]{:T(128)}, f32[1024]{0:T(1024)S(1)}, ...), condition=%wide.region_6.7_spmd.clone, body=%wide.region_3.6_spmd.clone.sunk | while | flops 273028096 | bytes 16319621 | solution.py:122
  85.2 2.7 multiply_reduce_fusion.3
  87.9 2.1 fusion.64
  90.0 0.1 copy-done.1
  90.1 1.5 convolution_add_fusion.2
  91.7 2.7 multiply_reduce_fusion.3
  94.3 2.1 fusion.64
  96.5 0.1 copy-done.1
  96.6 1.5 convolution_add_fusion.2
  98.1 2.7 multiply_reduce_fusion.3
  100.8 2.1 fusion.64
  102.9 0.1 copy-done.1
  103.0 1.5 convolution_add_fusion.2
  104.6 2.7 multiply_reduce_fusion.3
  107.3 2.1 fusion.64
  109.5 1.5 convolution_add_fusion.2
  111.1 2.7 multiply_reduce_fusion.3
  113.7 2.1 fusion.64
  116.0 1.5 convolution_add_fusion.2
  117.5 2.7 multiply_reduce_fusion.3
  120.2 2.1 fusion.64
  122.3 0.1 copy-done.1
  122.4 1.5 convolution_add_fusion.2
  124.0 2.7 multiply_reduce_fusion.3
  126.7 2.1 fusion.64
  128.8 0.1 copy-done.1
  128.9 1.5 convolution_add_fusion.2
  130.5 2.7 multiply_reduce_fusion.3
  133.1 2.1 fusion.64
  135.4 1.5 convolution_add_fusion.2
  136.9 0.2 divide_convert_fusion
  137.1 0.2 reshape.286
  137.3 1.7 convolution_convert_fusion
  139.1 0.7 all-gather.7.cloned.1.call-update
  139.8 0.5 all-gather.9.cloned.1.call-update
  140.4 0.5 all-gather.11.cloned.1.call-update
  140.9 0.2 reduce-scatter.2.cloned.1.call-start
  141.2 17.8 %all-reduce.3.cloned.1.call-done = (bf16[256,2048]{1,0:T(8,128)(2,1)}, bf16[256,2048]{1,0:T(8,128)(2,1)}) async-done(((bf16[256,2048]{1,0:T(8,128)(2,1)}, bf16[256,2048]{1,0:T(8,128)(2,1)}), (bf16[256,2048]{1,0:T(8,128)(2,1)}, bf16[256,2048]{1,0:T(8,128)(2,1)})) %all-reduce.3.cloned.1.call-update) | async-done | bytes 2097168 | tf_op jit(solution)/shard_map/psum | solution.py:137
  158.9 2.0 fusion.18
  161.0 95.3 %all-gather.7.cloned.1.call-done = bf16[2048,1536]{1,0:T(8,128)(2,1)} async-done(((bf16[128,1536]{1,0:T(8,128)(2,1)}), bf16[2048,1536]{1,0:T(8,128)(2,1)}) %all-gather.7.cloned.1.call-update) | async-done | bytes 6291472 | tf_op jit(solution)/shard_map/all_gather | solution.py:146
  256.3 94.6 %all-gather.9.cloned.1.call-done = bf16[2048,1536]{1,0:T(8,128)(2,1)} async-done(((bf16[128,1536]{1,0:T(8,128)(2,1)}), bf16[2048,1536]{1,0:T(8,128)(2,1)}) %all-gather.9.cloned.1.call-update) | async-done | bytes 6291472 | tf_op jit(solution)/shard_map/all_gather | solution.py:147
  350.9 9.8 %fusion.14 = f32[256,3072]{1,0:T(8,128)} fusion(bf16[2048,1536]{1,0:T(8,128)(2,1)} %all-gather.9.cloned.1.call-done, bf16[2048,1536]{1,0:T(8,128)(2,1)} %all-gather.7.cloned.1.call-done, bf16[256,2048]{1,0:T(8,128)(2,1)S(1)} %get-tuple-element.102, f32[2048]{0:T(1024)S(1)} %copy-done.4, f32[256]{0:T(256)S(1)} %add_rsqrt_fusion.1), kind=kOutput, calls=%fused_computation.20 | convolution fusion | flops 3248488448 | bytes 16786432 | tf_op jit(solution)/shard_map/dot_general | solution.py:151
  360.8 106.3 %all-gather.11.cloned.1.call-done = bf16[1536,2048]{1,0:T(8,128)(2,1)} async-done(((bf16[1536,128]{1,0:T(8,128)(2,1)}), bf16[1536,2048]{1,0:T(8,128)(2,1)}) %all-gather.11.cloned.1.call-update) | async-done | bytes 6291472 | tf_op jit(solution)/shard_map/all_gather | solution.py:155
  467.1 6.6 %convolution_convert_fusion.1 = bf16[256,2048]{1,0:T(8,128)(2,1)} fusion(bf16[1536,2048]{1,0:T(8,128)(2,1)} %all-gather.11.cloned.1.call-done, f32[256,3072]{1,0:T(8,128)} %fusion.14), kind=kOutput, calls=%fused_computation.27 | convolution fusion | flops 1613496320 | bytes 10485760 | tf_op jit(solution)/shard_map/dot_general | solution.py:153
  473.7 6.7 %reduce-scatter.2.cloned.1.call-done = bf16[128,2048]{1,0:T(8,128)(2,1)} async-done(((bf16[256,2048]{1,0:T(8,128)(2,1)}), bf16[128,2048]{1,0:T(8,128)(2,1)}) %reduce-scatter.2.cloned.1.call-update) | async-done | bytes 524304 | tf_op jit(solution)/shard_map/reduce_scatter | solution.py:158
  480.4 2.0 add_convert_fusion.1
  (61 shorter events, 0.8 us)
Async XLA Ops:
  6.5 130.8 %copy-start = (bf16[512,2048]{1,0:T(8,128)(2,1)S(1)}, bf16[512,2048]{1,0:T(8,128)(2,1)}, u32[]{:S(2)}) copy-start(bf16[512,2048]{1,0:T(8,128)(2,1)} %param.19) | copy-start | bytes 6291460
  6.5 5.7 %copy-start.3 = (f32[128]{0:T(128)S(1)}, f32[128]{0:T(128)}, u32[]{:S(2)}) copy-start(f32[128]{0:T(128)} %param.16) | copy-start | bytes 1540
  6.5 71.0 %all-gather.5.cloned.1.call-start = ((), (), s32[]{:S(2)}) async-start(), calls=%async_computation.1 | async-start | bytes 2228224 | tf_op jit(solution)/shard_map/all_gather | solution.py:110
  9.7 149.3 %all-reduce.3.cloned.1.call-start = ((), (), s32[]{:S(2)}) async-start(), calls=%async_computation.6 | async-start | bytes 4194304 | tf_op jit(solution)/shard_map/psum | solution.py:137
  13.5 2.0 copy-start.2
  87.9 2.2 copy-start.1
  94.3 2.2 copy-start.1
  100.8 2.2 copy-start.1
  107.3 2.2 copy-start.1
  113.7 2.2 copy-start.1
  120.2 2.2 copy-start.1
  126.7 2.2 copy-start.1
  133.1 2.2 copy-start.1
  139.0 211.9 %copy-start.4 = (f32[2048]{0:T(1024)S(1)}, f32[2048]{0:T(1024)}, u32[]{:S(2)}) copy-start(f32[2048]{0:T(1024)} %param.20) | copy-start | bytes 24580
  139.0 117.3 %all-gather.7.cloned.1.call-start = ((), (), s32[]{:S(2)}) async-start(), calls=%async_computation.2 | async-start | bytes 6684672 | tf_op jit(solution)/shard_map/all_gather | solution.py:146
  139.8 211.2 %all-gather.9.cloned.1.call-start = ((), (), s32[]{:S(2)}) async-start(), calls=%async_computation.3 | async-start | bytes 6684672 | tf_op jit(solution)/shard_map/all_gather | solution.py:147
  140.4 326.7 %all-gather.11.cloned.1.call-start = ((), (), s32[]{:S(2)}) async-start(), calls=%async_computation.4 | async-start | bytes 6684672 | tf_op jit(solution)/shard_map/all_gather | solution.py:155
  140.9 339.5 %reduce-scatter.2.cloned.1.call-start = ((), (), s32[]{:S(2)}) async-start(), calls=%async_computation.5 | async-start | bytes 1572864 | tf_op jit(solution)/shard_map/reduce_scatter | solution.py:158
Sparse Core Ops, SparseCore 0:
  10.1 67.4 all-gather.4
  139.1 19.7 all-reduce.2
  161.7 94.5 all-gather.6
  259.0 91.9 all-gather.8
  353.5 113.5 all-gather.10
  473.8 6.5 reduce-scatter.1
